TPU v7x, 512 devices: a whole 4x4x16 slice. The times are simulated.
512 devices in a mesh: fs: 16 (over y, x), tp: 32 (over z, core).
Axes of the slice: x: 4, y: 4, z: 16, core: 2. Of those that a mesh axis runs over, the one named last changes fastest.
Arguments:
- tokens: bfloat16 [8192, 2048], P('fs', 'tp'), may hold values from -6 to 6
- norm_gain: float32 [2048], P('fs'), may hold values from 0.1 to 1.9
- gate_train: float32 [2048, 8192], P('fs', 'tp'), may hold values from -0.125 to 0.125
- up_train: float32 [2048, 8192], P('fs', 'tp'), may hold values from -0.125 to 0.125
- down_train: float32 [8192, 2048], P('fs', 'tp'), may hold values from -0.0625 to 0.0625
Outputs:
- gate_serve: bfloat16 [2048, 8192], P(None, 'tp')
- up_serve: bfloat16 [2048, 8192], P(None, 'tp')
- down_serve: bfloat16 [8192, 2048], P('tp')
- layer_out: bfloat16 [8192, 2048], P(('fs', 'tp'))
All inputs are finite; a program needn't handle non-finite values.
Results may differ from a plain program's by a relative error of at most 0.024.
Values may be sent and summed in bfloat16 or wider, within the bound.
No kernel may reach another device: no remote copies, remote signals or barrier semaphores. Data moves between devices by JAX's collectives and lax.ppermute only.
A program may use at most 64 MiB of HBM per device.

v0:
```python
import jax
import jax.numpy as jnp
from jax import lax
from jax.sharding import Mesh
from jax.sharding import PartitionSpec as P

D = 2048
TP = ("tp_0", "tp_1")
FS_TP = ("fs", "tp_0", "tp_1")
epsilon = 1e-06


def side_by_side(arrays, axis, dim, along):
    both = jnp.concatenate(arrays, axis=along)
    whole, at, finished = (lax.all_gather(both, axis, axis=dim, tiled=True), 0, [])
    for a in arrays:
        finished.append(lax.slice_in_dim(whole, at, at + a.shape[along], axis=along))
        at += a.shape[along]
    return tuple(finished)


def joined_along(pieces, dim):
    shape = list(pieces.shape[1:])
    shape[dim] *= pieces.shape[0]
    return jnp.moveaxis(pieces, 0, dim).reshape(shape)


def copy_for_each(x, axis):
    copies = jnp.broadcast_to(x, (lax.axis_size(axis), *x.shape))
    return lax.all_to_all(copies, axis, split_axis=0, concat_axis=0, tiled=True)


def collect(x, axis, dim):
    return joined_along(copy_for_each(x, axis), dim)


def sum_in_order(pieces, axes, order):
    shape = [lax.axis_size(a) for a in axes]
    pieces = pieces.reshape(*shape, *pieces.shape[1:])
    pieces = pieces.transpose(*order, *range(len(axes), pieces.ndim))
    pieces = pieces.reshape(-1, *pieces.shape[len(axes) :])
    for k in order:
        pieces = lax.psum_scatter(pieces, axes[k], scatter_dimension=0, tiled=True)
    return pieces[0]


def cut_along(x, dim, count):
    before, after = (x.shape[:dim], x.shape[dim + 1 :])
    return jnp.moveaxis(x.reshape(*before, count, -1, *after), dim, 0)


def sum_by_axis(x, axes, order, dim):
    count = lax.axis_size(axes)
    return sum_in_order(cut_along(x, dim, count), axes, order)


def body(tokens, norm_gain, gate_train, up_train, down_train):
    gate_local = (norm_gain[:, None] * gate_train).astype(jnp.bfloat16)
    up_local = (norm_gain[:, None] * up_train).astype(jnp.bfloat16)
    down_local = down_train.astype(jnp.bfloat16)
    features = lax.all_gather(tokens, TP, axis=1, tiled=True)
    wide = features.astype(jnp.float32)
    squares = jnp.sum(wide * wide, axis=1)
    gate_whole, up_whole = side_by_side((gate_local, up_local), "fs", 0, 1)
    gate_sum = jnp.dot(features, gate_whole, preferred_element_type=jnp.float32)
    up_sum = jnp.dot(features, up_whole, preferred_element_type=jnp.float32)
    down_rows = collect(down_local, "fs", 0)
    down_whole = lax.all_to_all(down_rows, TP, split_axis=0, concat_axis=1, tiled=True)
    scale = lax.rsqrt(squares / D + epsilon)[:, None]
    hidden = (jax.nn.silu(gate_sum * scale) * (up_sum * scale)).astype(jnp.bfloat16)
    mixed = (
        sum_by_axis(
            jnp.dot(hidden, down_whole, preferred_element_type=jnp.float32).astype(jnp.bfloat16),
            TP,
            (1, 0),
            0,
        )
        .astype(jnp.float32)
        .astype(jnp.bfloat16)
    )
    return (gate_whole, up_whole, down_whole, mixed)


def solution(mesh):
    finer = Mesh(mesh.devices.reshape(mesh.shape["fs"], 16, 2), ("fs", "tp_0", "tp_1"))
    placed = (P("fs", TP), P("fs"), P("fs", TP), P("fs", TP), P("fs", TP))
    return jax.shard_map(
        body,
        mesh=finer,
        in_specs=placed,
        out_specs=(P(None, TP), P(None, TP), P(TP, None), P(FS_TP, None)),
        check_vma=False,
    )
```

profile of v0, /device:TPU:2, one launch (start us, length us, event | category | flops | bytes accessed | tf_op | source)
XLA Modules:
  0.0 262.0 jit_solution(8087558812155801704)
XLA Ops:
  7.2 0.0 all-gather.3.cloned.1.call-start
  7.2 1.1 multiply_convert_fusion.1
  8.3 0.7 pad_maximum_fusion
  8.9 0.0 all-gather.3.cloned.1.call-update
  9.0 0.9 convert_element_type.22
  9.9 1.1 broadcast_in_dim.2
  11.0 9.3 %all-to-all-start = ((bf16[16,512,64]{1,2,0:T(8,128)(2,1)}), bf16[16,512,64]{1,2,0:T(8,128)(2,1)S(1)}, u32[]{:S(2)}, u32[]{:S(2)}) async-start(bf16[16,512,64]{1,2,0:T(8,128)(2,1)} %broadcast_in_dim.2), calls=%async_computation | async-start | bytes 2097152 | tf_op jit(solution)/shard_map/all_to_all | solution.py:30
  20.3 0.0 all-gather.5.cloned.1.call-start
  20.3 0.7 all-gather.5.cloned.1.call-update
  21.0 13.6 %all-to-all-done = bf16[16,512,64]{1,2,0:T(8,128)(2,1)S(1)} async-done(((bf16[16,512,64]{1,2,0:T(8,128)(2,1)}), bf16[16,512,64]{1,2,0:T(8,128)(2,1)S(1)}, u32[]{:S(2)}, u32[]{:S(2)}) %all-to-all-start) | async-done | bytes 1048608 | tf_op jit(solution)/shard_map/all_to_all | solution.py:30
  34.7 0.6 copy.14
  35.2 0.4 all_to_all.18
  35.6 1.6 copy.15
  37.2 15.0 %all-to-all-start.1 = ((bf16[32,256,64]{1,2,0:T(8,128)(2,1)}), bf16[32,256,64]{1,2,0:T(8,128)(2,1)S(1)}, u32[]{:S(2)}, u32[]{:S(2)}) async-start(bf16[32,256,64]{1,2,0:T(8,128)(2,1)} %copy.15), calls=%async_computation.1 | async-start | bytes 2097152 | tf_op jit(solution)/shard_map/all_to_all | solution.py:68
  52.3 0.0 reduce-scatter.3.cloned.1.call-start
  52.3 23.6 %all-gather.3.cloned.1.call-done = bf16[2048,512]{1,0:T(8,128)(2,1)} async-done(((bf16[128,512]{1,0:T(8,128)(2,1)}), bf16[2048,512]{1,0:T(8,128)(2,1)}) %all-gather.3.cloned.1.call-update) | async-done | bytes 2097168 | tf_op jit(solution)/shard_map/all_gather | solution.py:15
  75.9 3.0 %fusion.12 = (bf16[2048,256]{1,0:T(8,128)(2,1)}, bf16[2048,256]{1,0:T(8,128)(2,1)}) fusion(bf16[2048,512]{1,0:T(8,128)(2,1)} %all-gather.3.cloned.1.call-done), kind=kLoop, calls=%fused_computation.20 | loop fusion | bytes 4194304 | tf_op jit(solution)/shard_map/slice | solution.py:17
  78.9 71.5 %all-gather.5.cloned.1.call-done = bf16[512,2048]{0,1:T(8,128)(2,1)} async-done(((bf16[512,64]{0,1:T(8,128)(2,1)}), bf16[512,2048]{0,1:T(8,128)(2,1)}) %all-gather.5.cloned.1.call-update) | async-done | bytes 2097168 | tf_op jit(solution)/shard_map/all_gather | solution.py:61
  150.4 0.0 copy-start
  150.4 2.2 multiply_reduce_fusion
  152.7 0.0 copy-done
  152.7 2.8 %fusion.2 = f32[512,256]{0,1:T(8,128)} fusion(bf16[2048,256]{1,0:T(8,128)(2,1)} %get-tuple-element.13, bf16[512,2048]{0,1:T(8,128)(2,1)S(1)} %copy-done, f32[512]{0:T(512)S(1)} %add_rsqrt_fusion), kind=kOutput, calls=%fused_computation.6 | convolution fusion | flops 537001984 | bytes 3672064 | tf_op jit(solution)/shard_map/dot_general | solution.py:65
  155.5 0.0 all-to-all-done.1
  155.5 4.2 %convolution_convert_fusion = bf16[512,2048]{1,0:T(8,128)(2,1)} fusion(bf16[256,2048]{0,1:T(8,128)(2,1)S(1)} %bitcast.26, bf16[2048,256]{1,0:T(8,128)(2,1)} %get-tuple-element.12, bf16[512,2048]{0,1:T(8,128)(2,1)S(1)} %copy-done, f32[512,256]{0,1:T(8,128)} %fusion.2, f32[512]{0:T(512)S(1)} %add_rsqrt_fusion), kind=kOutput, calls=%fused_computation.1 | convolution fusion | flops 1075707904 | bytes 6817792 | tf_op jit(solution)/shard_map/dot_general | solution.py:73
  159.7 3.2 %copy.16 = bf16[2,16,16,2048]{3,2,1,0:T(8,128)(2,1)} copy(bf16[2,16,16,2048]{3,2,0,1:T(8,128)(2,1)} %bitcast.28) | data formatting | bytes 4194304 | tf_op jit(solution)/shard_map/transpose | solution.py:40
  162.8 0.0 reduce-scatter.3.cloned.1.call-update
  162.8 0.0 reduce-scatter.5.cloned.1.call-start
  162.9 16.7 %reduce-scatter.3.cloned.1.call-done = bf16[16,16,2048]{2,1,0:T(8,128)(2,1)} async-done(((bf16[32,16,2048]{2,1,0:T(8,128)(2,1)}), bf16[16,16,2048]{2,1,0:T(8,128)(2,1)}) %reduce-scatter.3.cloned.1.call-update) | async-done | bytes 1048592 | tf_op jit(solution)/shard_map/reduce_scatter | solution.py:43
  179.6 0.0 reduce-scatter.5.cloned.1.call-update
  179.6 1.4 copy.17
  181.0 74.5 %reduce-scatter.5.cloned.1.call-done = bf16[1,16,2048]{2,1,0:T(8,128)(2,1)} async-done(((bf16[16,16,2048]{2,1,0:T(8,128)(2,1)}), bf16[1,16,2048]{2,1,0:T(8,128)(2,1)}) %reduce-scatter.5.cloned.1.call-update) | async-done | bytes 65552 | tf_op jit(solution)/shard_map/reduce_scatter | solution.py:43
  (1 shorter events, 0.0 us)
Async XLA Ops:
  7.2 68.8 %all-gather.3.cloned.1.call-start = ((), (), s32[]{:S(2)}) async-start(), calls=%async_computation.4 | async-start | bytes 2228224 | tf_op jit(solution)/shard_map/all_gather | solution.py:15
  11.0 23.7 %all-to-all-start = ((bf16[16,512,64]{1,2,0:T(8,128)(2,1)}), bf16[16,512,64]{1,2,0:T(8,128)(2,1)S(1)}, u32[]{:S(2)}, u32[]{:S(2)}) async-start(bf16[16,512,64]{1,2,0:T(8,128)(2,1)} %broadcast_in_dim.2), calls=%async_computation | async-start | bytes 2097152 | tf_op jit(solution)/shard_map/all_to_all | solution.py:30
  20.3 130.1 %all-gather.5.cloned.1.call-start = ((), (), s32[]{:S(2)}) async-start(), calls=%async_computation.5 | async-start | bytes 2162688 | tf_op jit(solution)/shard_map/all_gather | solution.py:61
  37.2 118.3 %all-to-all-start.1 = ((bf16[32,256,64]{1,2,0:T(8,128)(2,1)}), bf16[32,256,64]{1,2,0:T(8,128)(2,1)S(1)}, u32[]{:S(2)}, u32[]{:S(2)}) async-start(bf16[32,256,64]{1,2,0:T(8,128)(2,1)} %copy.15), calls=%async_computation.1 | async-start | bytes 2097152 | tf_op jit(solution)/shard_map/all_to_all | solution.py:68
  52.3 127.3 %reduce-scatter.3.cloned.1.call-start = ((), (), s32[]{:S(2)}) async-start(), calls=%async_computation.6 | async-start | bytes 3145728 | tf_op jit(solution)/shard_map/reduce_scatter | solution.py:43
  150.4 2.3 copy-start
  162.8 92.6 %reduce-scatter.5.cloned.1.call-start = ((), (), s32[]{:S(2)}) async-start(), calls=%async_computation.7 | async-start | bytes 1114112 | tf_op jit(solution)/shard_map/reduce_scatter | solution.py:43
Sparse Core Ops, SparseCore 0:
  11.6 64.3 all-gather.2
  78.1 72.3 all-gather.4
  163.0 16.5 reduce-scatter.2
  182.8 72.6 reduce-scatter.4
where the time goes:
time: 262 us
  waiting for transfers between devices  201 us (77%)
  starting transfers between devices  24.5 us (9%)
  between operations  13.8 us (5%)
  local copies, waits for them, and re-layouts  11.2 us (4%)
  matrix products  6.97 us (3%)
  other arithmetic  4.91 us (2%)
    reduce_scatter x2, waiting for transfers between devices, sum_in_order(): pieces = lax.psum_scatter(pieces, axes[k], scatter_dimension=0, tiled=True)  91.2 us
    all_gather x1, waiting for transfers between devices, body(): features = lax.all_gather(tokens, TP, axis=1, tiled=True)  71.5 us
    all_gather x1, waiting for transfers between devices, side_by_side(): lax.all_gather(both, axis, axis=dim, tiled=True)  23.6 us
    all_to_all x1, starting transfers between devices, body(): lax.all_to_all(down_rows, TP, split_axis=0, concat_axis=1, tiled=True)  15 us
    all_to_all x1, waiting for transfers between devices, copy_for_each(): return lax.all_to_all(copies, axis, split_axis=0, concat_axis=0, tiled=True)  13.6 us
    all_to_all x1, starting transfers between devices, copy_for_each(): return lax.all_to_all(copies, axis, split_axis=0, concat_axis=0, tiled=True)  9.32 us
  transfers between devices with their start and end apart: 6, of which 5 were waited for; matrix products, arithmetic and copies ran while one was open for 5% of the time, Pallas kernels for 0%

commit v1 on v0

--- a/solution.py
+++ b/solution.py
@@ -58,7 +58,8 @@
     gate_local = (norm_gain[:, None] * gate_train).astype(jnp.bfloat16)
     up_local = (norm_gain[:, None] * up_train).astype(jnp.bfloat16)
     down_local = down_train.astype(jnp.bfloat16)
-    features = lax.all_gather(tokens, TP, axis=1, tiled=True)
+    outgoing = jnp.stack([tokens] * lax.axis_size(TP))
+    features = jnp.concatenate(lax.all_to_all(outgoing, TP, 0, 0), axis=1)
     wide = features.astype(jnp.float32)
     squares = jnp.sum(wide * wide, axis=1)
     gate_whole, up_whole = side_by_side((gate_local, up_local), "fs", 0, 1)

time: 262 us -> 308 us (1.18)
  waiting for transfers between devices: 201 us -> 228 us
  blocking collectives: 0 us -> 23.2 us
  starting transfers between devices: 24.5 us -> 20.4 us
    all_to_all x1, waiting for transfers between devices: 13.6 us -> 93.6 us  [body(): features = jnp.concatenate(lax.all_to_all(outgoing, TP, 0, 0), axis=1)]
    all_gather x1 -> x0, waiting for transfers between devices: 71.5 us -> none  [body(): features = lax.all_gather(tokens, TP, axis=1, tiled=True)]
    all_to_all x1, waiting for transfers between devices: 0.01 us -> 50.8 us  [body(): lax.all_to_all(down_rows, TP, split_axis=0, concat_axis=1, tiled=True)]
    all_gather x1, waiting for transfers between devices: 23.6 us -> 0.02 us  [side_by_side(): lax.all_gather(both, axis, axis=dim, tiled=True)]
    all_to_all x0 -> x1, blocking collectives: none -> 23.2 us  [copy_for_each(): return lax.all_to_all(copies, axis, split_axis=0, concat_axis=0, tiled=True)]
    all_to_all x1, starting transfers between devices: 15 us -> 4.77 us  [body(): lax.all_to_all(down_rows, TP, split_axis=0, concat_axis=1, tiled=True)]
    reduce_scatter x2, waiting for transfers between devices: 91.2 us -> 83.9 us  [sum_in_order(): pieces = lax.psum_scatter(pieces, axes[k], scatter_dimension=0, tiled=True)]
    all_to_all x1, starting transfers between devices: 9.32 us -> 15.5 us  [body(): features = jnp.concatenate(lax.all_to_all(outgoing, TP, 0, 0), axis=1)]
  transfers between devices with their start and end apart: 6 -> 5, of which waited for: 5 -> 4; matrix products, arithmetic and copies ran while one was open for 5% -> 3% of each run, Pallas kernels for 0% -> 0%
where the time goes in v1:
time: 308 us
  waiting for transfers between devices  228 us (74%)
  blocking collectives  23.2 us (8%)
  starting transfers between devices  20.4 us (7%)
  local copies, waits for them, and re-layouts  13.8 us (4%)
  between operations  13.8 us (4%)
  matrix products  5.72 us (2%)
    all_to_all x1, waiting for transfers between devices, body(): features = jnp.concatenate(lax.all_to_all(outgoing, TP, 0, 0), axis=1)  93.6 us
    reduce_scatter x2, waiting for transfers between devices, sum_in_order(): pieces = lax.psum_scatter(pieces, axes[k], scatter_dimension=0, tiled=True)  83.9 us
    all_to_all x1, waiting for transfers between devices, body(): lax.all_to_all(down_rows, TP, split_axis=0, concat_axis=1, tiled=True)  50.8 us
    all_to_all x1, blocking collectives, copy_for_each(): return lax.all_to_all(copies, axis, split_axis=0, concat_axis=0, tiled=True)  23.2 us
    all_to_all x1, starting transfers between devices, body(): features = jnp.concatenate(lax.all_to_all(outgoing, TP, 0, 0), axis=1)  15.5 us
  transfers between devices with their start and end apart: 5, of which 4 were waited for; matrix products, arithmetic and copies ran while one was open for 3% of the time, Pallas kernels for 0%

profile of v1, /device:TPU:2, one launch (start us, length us, event | category | flops | bytes accessed | tf_op | source)
XLA Modules:
  0.0 307.5 jit_solution(10498873877991649862)
XLA Ops:
  7.2 0.0 copy-start.3
  7.2 0.9 convert_element_type.23
  8.1 0.1 broadcast_in_dim.2
  8.2 23.2 %all_to_all.29 = bf16[16,512,64]{1,2,0:T(8,128)(2,1)S(1)} all-to-all(bf16[16,512,64]{1,2,0:T(8,128)(2,1)S(1)} %broadcast_in_dim.2), channel_id=1, replica_groups=mesh['fs'=16,'tp_0'=16,'tp_1'=2] {'fs'}, dimensions={0} | all-to-all | bytes 2097152 | tf_op jit(solution)/shard_map/all_to_all | solution.py:30
  31.4 0.0 copy-done.3
  31.4 1.6 stack.2
  32.9 15.5 %all-to-all-start.2 = ((bf16[32,512,64]{1,2,0:T(8,128)(2,1)}), bf16[32,512,64]{1,2,0:T(8,128)(2,1)S(1)}, u32[]{:S(2)}, u32[]{:S(2)}) async-start(bf16[32,512,64]{1,2,0:T(8,128)(2,1)} %stack.2), calls=%async_computation.2 | async-start | bytes 4194304 | tf_op jit(solution)/shard_map/all_to_all | solution.py:62
  48.5 0.0 all-gather.2.cloned.1.call-start
  48.5 0.0 copy-done.1
  48.5 0.1 multiply_convert_fusion.1
  48.6 0.7 pad_maximum_fusion
  49.3 0.0 all-gather.2.cloned.1.call-update
  49.3 1.5 copy.15
  50.9 1.4 all_to_all.21
  52.3 1.6 copy.16
  53.9 93.6 %all-to-all-done.2 = bf16[32,512,64]{1,2,0:T(8,128)(2,1)S(1)} async-done(((bf16[32,512,64]{1,2,0:T(8,128)(2,1)}), bf16[32,512,64]{1,2,0:T(8,128)(2,1)S(1)}, u32[]{:S(2)}, u32[]{:S(2)}) %all-to-all-start.2) | async-done | bytes 2097184 | tf_op jit(solution)/shard_map/all_to_all | solution.py:62
  147.4 4.8 %all-to-all-start.1 = ((bf16[32,256,64]{1,2,0:T(8,128)(2,1)}), bf16[32,256,64]{1,2,0:T(8,128)(2,1)S(1)}, u32[]{:S(2)}, u32[]{:S(2)}) async-start(bf16[32,256,64]{1,2,0:T(8,128)(2,1)} %copy.16), calls=%async_computation.1 | async-start | bytes 2097152 | tf_op jit(solution)/shard_map/all_to_all | solution.py:69
  152.2 0.0 reduce-scatter.3.cloned.1.call-start
  152.3 0.0 all-gather.2.cloned.1.call-done
  152.3 2.6 fusion.12
  154.9 0.6 multiply_reduce_fusion
  155.5 0.4 copy-done
  155.9 1.5 fusion.2
  157.4 50.8 %all-to-all-done.1 = bf16[32,256,64]{1,2,0:T(8,128)(2,1)S(1)} async-done(((bf16[32,256,64]{1,2,0:T(8,128)(2,1)}), bf16[32,256,64]{1,2,0:T(8,128)(2,1)S(1)}, u32[]{:S(2)}, u32[]{:S(2)}) %all-to-all-start.1) | async-done | bytes 1048608 | tf_op jit(solution)/shard_map/all_to_all | solution.py:69
  208.2 4.2 %convolution_convert_fusion = bf16[512,2048]{1,0:T(8,128)(2,1)} fusion(bf16[256,2048]{0,1:T(8,128)(2,1)S(1)} %bitcast.32, bf16[2048,256]{1,0:T(8,128)(2,1)} %get-tuple-element.12, bf16[512,2048]{0,1:T(8,128)(2,1)S(1)} %bitcast.30, f32[512,256]{0,1:T(8,128)} %fusion.2, f32[512]{0:T(512)S(1)} %add_rsqrt_fusion), kind=kOutput, calls=%fused_computation.1 | convolution fusion | flops 1075707904 | bytes 6817792 | tf_op jit(solution)/shard_map/dot_general | solution.py:74
  212.4 3.2 %copy.17 = bf16[2,16,16,2048]{3,2,1,0:T(8,128)(2,1)} copy(bf16[2,16,16,2048]{3,2,0,1:T(8,128)(2,1)} %bitcast.34) | data formatting | bytes 4194304 | tf_op jit(solution)/shard_map/transpose | solution.py:40
  215.6 0.0 reduce-scatter.3.cloned.1.call-update
  215.6 0.0 reduce-scatter.5.cloned.1.call-start
  215.6 9.2 %reduce-scatter.3.cloned.1.call-done = bf16[16,16,2048]{2,1,0:T(8,128)(2,1)} async-done(((bf16[32,16,2048]{2,1,0:T(8,128)(2,1)}), bf16[16,16,2048]{2,1,0:T(8,128)(2,1)}) %reduce-scatter.3.cloned.1.call-update) | async-done | bytes 1048592 | tf_op jit(solution)/shard_map/reduce_scatter | solution.py:43
  224.9 0.0 reduce-scatter.5.cloned.1.call-update
  224.9 1.4 copy.18
  226.3 74.6 %reduce-scatter.5.cloned.1.call-done = bf16[1,16,2048]{2,1,0:T(8,128)(2,1)} async-done(((bf16[16,16,2048]{2,1,0:T(8,128)(2,1)}), bf16[1,16,2048]{2,1,0:T(8,128)(2,1)}) %reduce-scatter.5.cloned.1.call-update) | async-done | bytes 65552 | tf_op jit(solution)/shard_map/reduce_scatter | solution.py:43
  (7 shorter events, 0.0 us)
Async XLA Ops:
  7.2 24.2 %copy-start.3 = (bf16[512,64]{0,1:T(8,128)(2,1)S(1)}, bf16[512,64]{0,1:T(8,128)(2,1)}, u32[]{:S(2)}) copy-start(bf16[512,64]{0,1:T(8,128)(2,1)} %param.5) | copy-start | bytes 196612
  32.9 15.6 %copy-start.1 = (f32[128,256]{1,0:T(8,128)S(1)}, f32[128,256]{1,0:T(8,128)}, u32[]{:S(2)}) copy-start(f32[128,256]{1,0:T(8,128)} %param.7) | copy-start | bytes 393220
  32.9 15.6 %copy-start.2 = (f32[128,256]{1,0:T(8,128)S(1)}, f32[128,256]{1,0:T(8,128)}, u32[]{:S(2)}) copy-start(f32[128,256]{1,0:T(8,128)} %param.8) | copy-start | bytes 393220
  32.9 15.6 %copy-start.4 = (f32[128]{0:T(128)S(1)}, f32[128]{0:T(128)}, u32[]{:S(2)}) copy-start(f32[128]{0:T(128)} %param.6) | copy-start | bytes 1540
  32.9 114.5 %all-to-all-start.2 = ((bf16[32,512,64]{1,2,0:T(8,128)(2,1)}), bf16[32,512,64]{1,2,0:T(8,128)(2,1)S(1)}, u32[]{:S(2)}, u32[]{:S(2)}) async-start(bf16[32,512,64]{1,2,0:T(8,128)(2,1)} %stack.2), calls=%async_computation.2 | async-start | bytes 4194304 | tf_op jit(solution)/shard_map/all_to_all | solution.py:62
  48.5 103.8 %all-gather.2.cloned.1.call-start = ((), (), s32[]{:S(2)}) async-start(), calls=%async_computation.5 | async-start | bytes 2228224 | tf_op jit(solution)/shard_map/all_gather | solution.py:15
  147.4 60.8 %all-to-all-start.1 = ((bf16[32,256,64]{1,2,0:T(8,128)(2,1)}), bf16[32,256,64]{1,2,0:T(8,128)(2,1)S(1)}, u32[]{:S(2)}, u32[]{:S(2)}) async-start(bf16[32,256,64]{1,2,0:T(8,128)(2,1)} %copy.16), calls=%async_computation.1 | async-start | bytes 2097152 | tf_op jit(solution)/shard_map/all_to_all | solution.py:69
  152.2 72.7 %reduce-scatter.3.cloned.1.call-start = ((), (), s32[]{:S(2)}) async-start(), calls=%async_computation.6 | async-start | bytes 3145728 | tf_op jit(solution)/shard_map/reduce_scatter | solution.py:43
  154.9 1.0 copy-start
  215.6 85.4 %reduce-scatter.5.cloned.1.call-start = ((), (), s32[]{:S(2)}) async-start(), calls=%async_computation.7 | async-start | bytes 1114112 | tf_op jit(solution)/shard_map/reduce_scatter | solution.py:43
Sparse Core Ops, SparseCore 0:
  52.9 58.0 all-gather.1
  215.7 9.1 reduce-scatter.2
  228.3 72.6 reduce-scatter.4
